TPU v7x, 32 devices: a whole 2x2x4 slice. The times are simulated.
32 devices in a mesh: row: 8 (over z, x), col: 4 (over y, core).
Axes of the slice: x: 2, y: 2, z: 4, core: 2. Of those that a mesh axis runs over, the one named last changes fastest.
Arguments:
- tokens: bfloat16 [16384, 4096], P(('row', 'col')), may hold values from -36 to 36
- norm_gain: bfloat16 [4096], replicated, may hold values from 0.099609375 to 1.8984375
- in_weight: bfloat16 [4096, 1024], replicated, may hold values from -0.09375 to 0.09375
- out_weight: bfloat16 [1024, 4096], replicated, may hold values from -0.1875 to 0.1875
Outputs:
- mixed: bfloat16 [16384, 4096], P(('row', 'col'))
All inputs are finite; a program needn't handle non-finite values.
Results may differ from a plain program's by a relative error of at most 0.0071.
Values may be sent and summed in bfloat16 or wider, within the bound.
A program may use at most 128 MiB of HBM per device.

v0:
```python
import functools
import math

import jax
import jax.numpy as jnp
import numpy as np
from jax import lax
from jax.experimental import pallas as pl
from jax.experimental.pallas import tpu as pltpu
from jax.sharding import PartitionSpec as P

GROUP_WIDTH = 64
AXES = ("row", "col")


def channel_tables(slots):
    pairs = slots // 2
    half = GROUP_WIDTH // 2
    index = np.arange(GROUP_WIDTH)
    forward = np.zeros((GROUP_WIDTH, GROUP_WIDTH))
    order = np.zeros((GROUP_WIDTH, GROUP_WIDTH))
    for slot in range(GROUP_WIDTH):
        place, within = divmod(slot, slots)
        pair = place * pairs + within % pairs
        angles = 2.0 * math.pi / GROUP_WIDTH * (pair * index % GROUP_WIDTH)
        if within < pairs:
            forward[slot] = np.cos(angles)
            order[pair, slot] = 1.0
        elif pair == 0:
            forward[slot] = np.cos(math.pi * index)
            order[half, slot] = 1.0
        else:
            forward[slot] = np.sin(angles)
            order[GROUP_WIDTH - pair, slot] = 1.0
    forward /= math.sqrt(GROUP_WIDTH)
    return forward.astype(jnp.bfloat16), order.astype(jnp.bfloat16)


def position_tables(outer, inner, devices):
    length = outer * inner
    k1 = np.arange(outer)
    n2 = np.arange(inner)
    n1_order = k1.reshape(devices, -1).T.reshape(-1)
    k2_order = n2.reshape(devices, -1).T.reshape(-1)
    one = 2.0 * math.pi / outer * (np.outer(n1_order, k1) % outer)
    first = np.concatenate([np.cos(one), -np.sin(one)], axis=1)
    turn = 2.0 * math.pi / length * np.outer(n2, k1)
    two = 2.0 * math.pi / inner * (np.outer(k2_order, n2) % inner)
    scale = 1.0 / math.sqrt(length)
    c, s, z = np.cos(two) * scale, np.sin(two) * scale, np.zeros((inner, inner))
    usual = np.block([[c, s, -s, c], [c, s, s, -c]])
    zeroth = np.block([[c, s, z, z], [z, z, c, s]])
    return (
        first.astype(jnp.bfloat16),
        np.cos(turn).astype(np.float32),
        np.sin(turn).astype(np.float32),
        usual.astype(jnp.bfloat16),
        zeroth.astype(jnp.bfloat16),
    )


PLANES = 4
MESH = pl.DeviceIdType.MESH


def place_of(device, columns):
    return (device // columns, device % columns)


def turned_plane(plane, step):
    high = (plane // 2 + 1 - step // 2) % 2
    low = (plane % 2 + (step + 1) // 2) % 2
    return 2 * high + low


def here(devices):
    columns = lax.axis_size("col")
    me = lax.axis_index("row") * columns + lax.axis_index("col")
    per = devices // PLANES
    return me, columns, per, me // per, me % per


def greet(devices):
    me, columns, _, _, _ = here(devices)
    barrier = pltpu.get_barrier_semaphore()

    def signal(step, carry):
        other = (me + step) % devices
        pl.semaphore_signal(barrier, inc=1, device_id=place_of(other, columns), device_id_type=MESH)
        return carry

    lax.fori_loop(1, devices, signal, 0)
    return lambda: pl.semaphore_wait(barrier, devices - 1)


def send_plane(devices, step, from_ref, to_ref, send_sem, recv_sem, first):
    me, columns, per, plane, lane = here(devices)
    target_plane = turned_plane(plane, step)

    def send(hop, carry):
        target = target_plane * per + (lane + hop) % per
        pltpu.make_async_remote_copy(
            src_ref=from_ref.at[target],
            dst_ref=to_ref.at[me],
            send_sem=send_sem,
            recv_sem=recv_sem,
            device_id=place_of(target, columns),
            device_id_type=MESH,
        ).start()
        return carry

    lax.fori_loop(first, per, send, 0)


def wait_for(ref, sem, count):
    part = ref.at[pl.ds(0, count)]
    pltpu.make_async_copy(part, part, sem).wait()


def enter_kernel(
    devices, tokens, gain, weight, forward, out, raw, normed, held, sent, wide, token_sem, weight_sem, own_sem, send_sem, recv_sem
):
    me, columns, per, plane, lane = here(devices)
    pieces = token_sem.shape[0]
    rows = raw.shape[0]
    piece = rows // pieces
    width = held.shape[2]

    def token_copy(index):
        part = pl.ds(index * piece, piece)
        return pltpu.make_async_copy(tokens.at[part], raw.at[part], token_sem.at[index])

    def weight_copy(step):
        target_plane = turned_plane(plane, step)
        part = pl.ds(pl.multiple_of(target_plane * width, width), width)
        return pltpu.make_async_copy(weight.at[:, part], held.at[step], weight_sem.at[step])

    for index in range(pieces):
        token_copy(index).start()
    for step in range(PLANES):
        weight_copy(step).start()
    arrive = greet(devices)

    wide[...] = gain[...].astype(jnp.float32).reshape(wide.shape)
    block = 16
    for index in range(pieces):
        token_copy(index).wait()

        def normalise(number, carry):
            part = pl.ds(pl.multiple_of(index * piece + number * block, block), block)
            floats = raw[part, :].astype(jnp.float32)
            scaling = lax.rsqrt(jnp.mean(floats * floats, axis=-1, keepdims=True) + 1e-06)
            normed[part, :] = (floats * scaling * wide[...]).astype(jnp.bfloat16)
            return carry

        lax.fori_loop(0, piece // block, normalise, 0)

    arrive()

    def chunk(step, carry):
        weight_copy(step).wait()
        target_plane = turned_plane(plane, step)
        hidden = jnp.dot(normed[...], held[step], preferred_element_type=jnp.float32).astype(jnp.bfloat16)
        spectrum = lax.dot_general(
            forward[...], hidden, (((1,), (1,)), ((), ())), preferred_element_type=jnp.float32
        )
        sent[pl.ds(target_plane * per, per)] = spectrum.reshape(per, width // per, rows).astype(jnp.bfloat16)
        send_plane(devices, step, sent, out, send_sem.at[step], recv_sem.at[step], step // (PLANES - 1))
        return carry

    lax.fori_loop(0, PLANES, chunk, 0)
    own = pltpu.make_async_copy(sent.at[me], out.at[me], own_sem)
    own.start()
    finish(per, sent, send_sem)
    finish(per, sent, recv_sem)
    own.wait()


def finish(per, ref, sem):
    for step in range(PLANES):
        wait_for(ref, sem.at[step], per - step // (PLANES - 1))


def enter(tokens, gain, weight, forward, devices):
    rows, depth = tokens.shape
    channels = weight.shape[1]
    slots = channels // devices
    whole = pl.BlockSpec(memory_space=pltpu.VMEM)
    hbm = pl.BlockSpec(memory_space=pltpu.HBM)
    pieces = 4
    return pl.pallas_call(
        functools.partial(enter_kernel, devices),
        out_shape=jax.ShapeDtypeStruct((devices, slots, rows), jnp.bfloat16),
        in_specs=[hbm, whole, hbm, whole],
        out_specs=pl.BlockSpec(memory_space=pl.ANY),
        scratch_shapes=[
            pltpu.VMEM((rows, depth), jnp.bfloat16),
            pltpu.VMEM((rows, depth), jnp.bfloat16),
            pltpu.VMEM((PLANES, depth, channels // PLANES), jnp.bfloat16),
            pltpu.VMEM((devices, slots, rows), jnp.bfloat16),
            pltpu.VMEM((1, depth), jnp.float32),
            pltpu.SemaphoreType.DMA((pieces,)),
            pltpu.SemaphoreType.DMA((PLANES,)),
            pltpu.SemaphoreType.DMA,
            pltpu.SemaphoreType.DMA((PLANES,)),
            pltpu.SemaphoreType.DMA((PLANES,)),
        ],
        compiler_params=pltpu.CompilerParams(collective_id=0, has_side_effects=True, vmem_limit_bytes=61 << 20),
    )(tokens, gain, weight, forward)


def leave_kernel(
    devices,
    taken,
    first,
    turn_cos,
    turn_sin,
    usual,
    special,
    order,
    out,
    table,
    grid,
    done,
    back,
    landed,
    own_sem,
    send_sem,
    recv_sem,
):
    me, columns, per, plane, lane = here(devices)
    arrive = greet(devices)
    units, _, slots, rows = back.shape
    pairs = slots // 2
    outer = first.shape[0]
    inner = turn_cos.shape[0]

    def turned(slot):
        a = lax.dot_general(
            grid[slot], first[...], (((0,), (0,)), ((), ())), preferred_element_type=jnp.float32
        )
        re, im = a[:, :outer], a[:, outer:]
        c, s = turn_cos[...], turn_sin[...]
        return [(re * c + im * s).astype(jnp.bfloat16), (im * c - re * s).astype(jnp.bfloat16)]

    for unit in range(units):
        zeroth_here = ((me * units + unit) * pairs) % (GROUP_WIDTH // 2) == 0

        @pl.when(zeroth_here)
        def _():
            table[...] = special[...]

        @pl.when(jnp.logical_not(zeroth_here))
        def _():
            table[...] = usual[...]

        for part in range(outer // devices):
            block = taken[:, unit * slots : (unit + 1) * slots, part * inner : (part + 1) * inner]
            grid[:, part * devices : (part + 1) * devices, :] = jnp.swapaxes(
                block.astype(jnp.float32), 0, 1
            ).astype(jnp.bfloat16)
        for pair in range(pairs):
            b = jnp.concatenate(turned(pair) + turned(pair + pairs), axis=0)
            here_table = table if pair == 0 else usual
            o = jnp.dot(here_table[...], b, preferred_element_type=jnp.float32)
            done[pair] = o[:inner]
            done[pair + pairs] = o[inner:]
        for part in range(inner // devices):
            block = done[:, part * devices : (part + 1) * devices, :]
            back[unit, :, :, part * outer : (part + 1) * outer] = jnp.swapaxes(block, 0, 1).astype(jnp.bfloat16)
        if unit == 0:
            arrive()
        for step in range(PLANES):
            send_plane(
                devices,
                step,
                back.at[unit],
                landed.at[unit],
                send_sem.at[unit, step],
                recv_sem.at[unit, step],
                step // (PLANES - 1),
            )
        pltpu.make_async_copy(back.at[unit, me], landed.at[unit, me], own_sem.at[unit]).start()

    width = order.shape[0]
    for unit in range(units):
        pltpu.make_async_copy(back.at[unit, me], landed.at[unit, me], own_sem.at[unit]).wait()
    for number in range(PLANES):
        step = PLANES - 1 - number
        source = turned_plane(plane, step)
        parts = []
        for unit in range(units):
            wait_for(landed.at[unit], recv_sem.at[unit, step], per - step // (PLANES - 1))
        for unit in range(units):
            parts.append(landed[unit, pl.ds(source * per, per)].astype(jnp.float32))
        joined = jnp.concatenate(parts, axis=1).reshape(width, rows).astype(jnp.bfloat16)
        turned_back = lax.dot_general(
            joined, order[...], (((0,), (0,)), ((), ())), preferred_element_type=jnp.float32
        ).astype(jnp.bfloat16)
        out[:, pl.ds(pl.multiple_of(source * width, width), width)] = turned_back
    for unit in range(units):
        for step in range(PLANES):
            wait_for(back.at[unit], send_sem.at[unit, step], per - step // (PLANES - 1))


def leave(taken, tables, order, units, devices):
    _, all_slots, rows = taken.shape
    slots = all_slots // units
    outer = tables[0].shape[0]
    inner = tables[1].shape[0]
    whole = pl.BlockSpec(memory_space=pltpu.VMEM)
    return pl.pallas_call(
        functools.partial(leave_kernel, devices),
        out_shape=jax.ShapeDtypeStruct((rows, devices * all_slots), jnp.bfloat16),
        in_specs=[whole] * 7,
        out_specs=whole,
        scratch_shapes=[
            pltpu.VMEM(tables[3].shape, jnp.bfloat16),
            pltpu.VMEM((slots, outer, inner), jnp.bfloat16),
            pltpu.VMEM((slots, inner, outer), jnp.float32),
            pltpu.VMEM((units, devices, slots, rows), jnp.bfloat16),
            pltpu.VMEM((units, devices, slots, rows), jnp.bfloat16),
            pltpu.SemaphoreType.DMA((units,)),
            pltpu.SemaphoreType.DMA((units, PLANES)),
            pltpu.SemaphoreType.DMA((units, PLANES)),
        ],
        compiler_params=pltpu.CompilerParams(collective_id=1, has_side_effects=True, vmem_limit_bytes=20 << 20),
        cost_estimate=pl.CostEstimate(flops=20 * 10**9, bytes_accessed=50 * 2**20, transcendentals=0),
    )(taken, *tables, order)


def local(tokens, norm_gain, in_weight, out_weight):
    rows_here = tokens.shape[0]
    channels = in_weight.shape[1]
    devices = lax.axis_size(AXES)
    slots = channels // devices
    units = max(1, slots // 16)
    length = rows_here * devices
    inner = 1 << ((length.bit_length()) // 2)
    outer = length // inner

    forward, order = channel_tables(slots // units)
    several = np.eye(channels // PLANES // GROUP_WIDTH)
    forward = np.kron(several, forward.astype(np.float32)).astype(jnp.bfloat16)
    order = np.kron(several, order.astype(np.float32)).T.astype(jnp.bfloat16)
    taken = enter(tokens, norm_gain, in_weight, forward, devices)
    ordered = leave(taken, position_tables(outer, inner, devices), order, units, devices)
    return jnp.dot(ordered, out_weight, preferred_element_type=jnp.float32).astype(jnp.bfloat16)


def solution(mesh):
    placed = (P(AXES, None), P(), P(), P())
    return jax.shard_map(
        local, mesh=mesh, in_specs=placed, out_specs=P(AXES, None), check_vma=False
    )
```

profile of v0, /device:TPU:9, one launch (start us, length us, event | category | flops | bytes accessed | tf_op | source)
XLA Modules:
  0.0 70.2 jit_solution(12022248669264555876)
XLA Ops:
  0.0 0.0 copy-start.3
  0.0 0.0 copy-start.1
  0.0 0.0 copy-start.2
  0.0 0.0 copy-start.4
  0.0 0.0 copy-start.5
  0.0 0.0 copy-start.6
  0.0 34.4 %shard_map.109.taken = bf16[32,32,512]{2,1,0:T(8,128)(2,1)} custom-call(bf16[512,4096]{1,0:T(8,128)(2,1)} %tokens.1, bf16[4096]{0:T(1024)(128)(2,1)} %gain.1, bf16[4096,1024]{1,0:T(8,128)(2,1)} %weight.1, bf16[256,256]{1,0:T(8,128)(2,1)} %constant.14.clone.forward), custom_call_target="tpu_custom_call" | custom-call | tf_op jit(solution)/shard_map/pallas_call | solution.py:191
  34.5 0.0 copy-done.3
  34.5 0.0 copy-done.1
  34.5 0.0 copy-done.2
  34.5 0.0 copy-done.4
  34.5 0.0 copy-done.5
  34.6 0.0 copy-done.6
  34.6 0.0 copy-start
  34.6 1.2 %copy-done = bf16[32,32,512]{2,1,0:T(8,128)(2,1)S(1)} copy-done((bf16[32,32,512]{2,1,0:T(8,128)(2,1)S(1)}, bf16[32,32,512]{2,1,0:T(8,128)(2,1)}, u32[]{:S(2)}) %copy-start) | copy-done | bytes 1048600
  35.8 0.0 copy-start.7
  35.8 28.3 %shard_map.110 = bf16[512,1024]{1,0:T(8,128)(2,1)S(1)} custom-call(bf16[32,32,512]{2,1,0:T(8,128)(2,1)S(1)} %copy-done, bf16[128,256]{1,0:T(8,128)(2,1)S(1)} %copy-done.6, f32[128,128]{1,0:T(8,128)S(1)} %copy-done.5, f32[128,128]{1,0:T(8,128)S(1)} %copy-done.4, bf16[256,512]{1,0:T(8,128)(2,1)S(1)} %copy-done.2, bf16[256,512]{1,0:T(8,128)(2,1)S(1)} %copy-done.1, ...), custom_call_target="tpu_custom_call" | custom-call | flops 20000000000 | bytes 52428800 | tf_op jit(solution)/shard_map/pallas_call | solution.py:312
  64.1 0.0 copy-done.7
  64.1 6.1 %convolution_convert_fusion = bf16[512,4096]{1,0:T(8,128)(2,1)} fusion(bf16[512,1024]{1,0:T(8,128)(2,1)S(1)} %shard_map.110, bf16[1024,4096]{1,0:T(8,128)(2,1)S(1)} %copy-done.7), kind=kOutput, calls=%fused_computation | convolution fusion | flops 4297064448 | bytes 13631488 | tf_op jit(solution)/shard_map/dot_general | solution.py:348
Async XLA Ops:
  0.0 34.5 %copy-start.3 = (bf16[256,256]{1,0:T(8,128)(2,1)S(1)}, bf16[256,256]{1,0:T(8,128)(2,1)}, u32[]{:S(2)}) copy-start(bf16[256,256]{1,0:T(8,128)(2,1)} %constant.20.clone.order) | copy-start | bytes 393220
  0.0 34.5 %copy-start.1 = (bf16[256,512]{1,0:T(8,128)(2,1)S(1)}, bf16[256,512]{1,0:T(8,128)(2,1)}, u32[]{:S(2)}) copy-start(bf16[256,512]{1,0:T(8,128)(2,1)} %constant.19.clone.special) | copy-start | bytes 786436
  0.0 34.5 %copy-start.2 = (bf16[256,512]{1,0:T(8,128)(2,1)S(1)}, bf16[256,512]{1,0:T(8,128)(2,1)}, u32[]{:S(2)}) copy-start(bf16[256,512]{1,0:T(8,128)(2,1)} %constant.18.clone.usual) | copy-start | bytes 786436
  0.0 34.5 %copy-start.4 = (f32[128,128]{1,0:T(8,128)S(1)}, f32[128,128]{1,0:T(8,128)}, u32[]{:S(2)}) copy-start(f32[128,128]{1,0:T(8,128)} %constant.17.clone.turn_sin) | copy-start | bytes 196612
  0.0 34.5 %copy-start.5 = (f32[128,128]{1,0:T(8,128)S(1)}, f32[128,128]{1,0:T(8,128)}, u32[]{:S(2)}) copy-start(f32[128,128]{1,0:T(8,128)} %constant.16.clone.turn_cos) | copy-start | bytes 196612
  0.0 34.5 %copy-start.6 = (bf16[128,256]{1,0:T(8,128)(2,1)S(1)}, bf16[128,256]{1,0:T(8,128)(2,1)}, u32[]{:S(2)}) copy-start(bf16[128,256]{1,0:T(8,128)(2,1)} %constant.15.clone.first) | copy-start | bytes 196612
  34.6 1.2 %copy-start = (bf16[32,32,512]{2,1,0:T(8,128)(2,1)S(1)}, bf16[32,32,512]{2,1,0:T(8,128)(2,1)}, u32[]{:S(2)}) copy-start(bf16[32,32,512]{2,1,0:T(8,128)(2,1)} %shard_map.109.taken) | copy-start | bytes 3145732
  35.8 28.3 %copy-start.7 = (bf16[1024,4096]{1,0:T(8,128)(2,1)S(1)}, bf16[1024,4096]{1,0:T(8,128)(2,1)}, u32[]{:S(2)}) copy-start(bf16[1024,4096]{1,0:T(8,128)(2,1)} %param.14) | copy-start | bytes 25165828
where the time goes:
time: 70.3 us; the launch traced here: 70.2 us
  Pallas kernels  62.7 us (89%)
  matrix products  6.08 us (9%)
  local copies, waits for them, and re-layouts  1.25 us (2%)
    pallas_call x1, Pallas kernels, enter(): pl.pallas_call(functools.partial(enter_kernel, devices), out_shape=jax.Sh...  34.4 us
    pallas_call x1, Pallas kernels, leave(): pl.pallas_call(functools.partial(leave_kernel, devices), out_shape=jax.Sh...  28.3 us
    dot_general x1, matrix products, local(): jnp.dot(ordered, out_weight, preferred_element_type=jnp.float32)  6.08 us

commit v1 on v0

v1 whole, which is shorter than its diff:
```python
import functools
import math

import jax
import jax.numpy as jnp
import numpy as np
from jax import lax
from jax.experimental import pallas as pl
from jax.experimental.pallas import tpu as pltpu
from jax.sharding import PartitionSpec as P

GROUP_WIDTH = 64
AXES = ("row", "col")


def channel_tables(slots):
    pairs = slots // 2
    half = GROUP_WIDTH // 2
    index = np.arange(GROUP_WIDTH)
    forward = np.zeros((GROUP_WIDTH, GROUP_WIDTH))
    order = np.zeros((GROUP_WIDTH, GROUP_WIDTH))
    for slot in range(GROUP_WIDTH):
        place, within = divmod(slot, slots)
        pair = place * pairs + within % pairs
        angles = 2.0 * math.pi / GROUP_WIDTH * (pair * index % GROUP_WIDTH)
        if within < pairs:
            forward[slot] = np.cos(angles)
            order[pair, slot] = 1.0
        elif pair == 0:
            forward[slot] = np.cos(math.pi * index)
            order[half, slot] = 1.0
        else:
            forward[slot] = np.sin(angles)
            order[GROUP_WIDTH - pair, slot] = 1.0
    forward /= math.sqrt(GROUP_WIDTH)
    return forward.astype(jnp.bfloat16), order.astype(jnp.bfloat16)


def position_tables(outer, inner, devices):
    length = outer * inner
    k1 = np.arange(outer)
    n2 = np.arange(inner)
    n1_order = k1.reshape(devices, -1).T.reshape(-1)
    k2_order = n2.reshape(devices, -1).T.reshape(-1)
    one = 2.0 * math.pi / outer * (np.outer(n1_order, k1) % outer)
    first = np.concatenate([np.cos(one), -np.sin(one)], axis=1)
    turn = 2.0 * math.pi / length * np.outer(n2, k1)
    two = 2.0 * math.pi / inner * (np.outer(k2_order, n2) % inner)
    scale = 1.0 / math.sqrt(length)
    c, s, z = np.cos(two) * scale, np.sin(two) * scale, np.zeros((inner, inner))
    usual = np.block([[c, s, -s, c], [c, s, s, -c]])
    zeroth = np.block([[c, s, z, z], [z, z, c, s]])
    return (
        first.astype(jnp.bfloat16),
        np.cos(turn).astype(np.float32),
        np.sin(turn).astype(np.float32),
        usual.astype(jnp.bfloat16),
        zeroth.astype(jnp.bfloat16),
    )


PLANES = 4
HALVES = 2
LANES = 128
MESH = pl.DeviceIdType.MESH


def place_of(device, columns):
    return (device // columns, device % columns)


def turned_plane(plane, step):
    high = (plane // 2 + 1 - step // 2) % 2
    low = (plane % 2 + (step + 1) // 2) % 2
    return 2 * high + low


def here(devices):
    columns = lax.axis_size("col")
    me = lax.axis_index("row") * columns + lax.axis_index("col")
    per = devices // PLANES
    return me, columns, per, me // per, me % per


def greet(devices):
    me, columns, _, _, _ = here(devices)
    barrier = pltpu.get_barrier_semaphore()

    def signal(step, carry):
        other = (me + step) % devices
        pl.semaphore_signal(barrier, inc=1, device_id=place_of(other, columns), device_id_type=MESH)
        return carry

    lax.fori_loop(1, devices, signal, 0)
    return lambda: pl.semaphore_wait(barrier, devices - 1)


def send_plane(devices, step, from_ref, to_ref, send_sem, recv_sem, first):
    me, columns, per, plane, lane = here(devices)
    target_plane = turned_plane(plane, step)

    def send(hop, carry):
        target = target_plane * per + (lane + hop) % per
        pltpu.make_async_remote_copy(
            src_ref=from_ref.at[target],
            dst_ref=to_ref.at[me],
            send_sem=send_sem,
            recv_sem=recv_sem,
            device_id=place_of(target, columns),
            device_id_type=MESH,
        ).start()
        return carry

    lax.fori_loop(first, per, send, 0)


def wait_for(ref, sem, count):
    part = ref.at[pl.ds(0, count)]
    pltpu.make_async_copy(part, part, sem).wait()


def mixer_kernel(
    devices,
    tokens,
    weight,
    out_weight,
    gain_hbm,
    forward_hbm,
    first_hbm,
    turn_cos_hbm,
    turn_sin_hbm,
    usual_hbm,
    special_hbm,
    order_hbm,
    total,
    last,
    last_weight,
    gain,
    forward,
    first,
    turn_cos,
    turn_sin,
    usual,
    special,
    order,
    raw,
    held,
    held_out,
    wide,
    squares,
    sent,
    taken,
    table,
    grid,
    done,
    back,
    landed,
    ordered,
    token_sem,
    weight_sem,
    out_sem,
    last_sem,
    own_sem,
    send_sem,
    recv_sem,
    own_back_sem,
    back_sem,
    landed_sem,
    table_sem,
):
    me, columns, per, plane, lane = here(devices)
    pieces = token_sem.shape[0]
    rows, depth = raw.shape
    piece = rows // pieces
    width = held.shape[2]
    units, _, slots, _ = sent.shape
    members = devices // HALVES
    near = plane // HALVES
    far = (near + 1) % HALVES
    pairs = slots // 2
    places = GROUP_WIDTH // slots
    outer = first.shape[0]
    inner = turn_cos.shape[0]
    chunks = units * HALVES

    def token_copy(index):
        part = pl.ds(index * piece, piece)
        return pltpu.make_async_copy(tokens.at[part], raw.at[part], token_sem.at[index])

    def half_of(number):
        return (near + 1 + number) % HALVES

    def weight_copy(step):
        begin = pl.multiple_of((step // HALVES * HALVES + half_of(step % HALVES)) * width, width)
        return pltpu.make_async_copy(weight.at[:, pl.ds(begin, width)], held.at[step], weight_sem.at[step])

    out_width = out_weight.shape[1]
    far_begin = pl.multiple_of(((units - 1) * HALVES + far) * width, width)
    out_copy = pltpu.make_async_copy(out_weight, held_out, out_sem)
    last_copy = pltpu.make_async_copy(out_weight.at[pl.ds(far_begin, width)], last_weight, last_sem)

    distant = (gain_hbm, forward_hbm, first_hbm, turn_cos_hbm, turn_sin_hbm, usual_hbm, special_hbm, order_hbm)
    nearby = (gain, forward, first, turn_cos, turn_sin, usual, special, order)
    table_copies = [
        pltpu.make_async_copy(a, b, table_sem.at[index]) for index, (a, b) in enumerate(zip(distant, nearby))
    ]
    table_copies[0].start()
    for index in range(pieces):
        token_copy(index).start()
    weight_copy(0).start()
    table_copies[1].start()
    arrive = greet(devices)

    block = wide.shape[0]
    table_copies[0].wait()
    wide[...] = jnp.broadcast_to(gain[...].astype(jnp.float32).reshape(1, depth), wide.shape).astype(jnp.bfloat16)
    for index in range(pieces):
        token_copy(index).wait()

        def gather_squares(number, carry):
            part = pl.ds(pl.multiple_of(index * piece + number * block, block), block)
            parts = [jnp.zeros((block, LANES), jnp.float32) for _ in range(4)]
            for column in range(depth // LANES):
                across = pl.ds(column * LANES, LANES)
                values = raw[part, across]
                floats = values.astype(jnp.float32)
                parts[column % 4] = parts[column % 4] + floats * floats
                raw[part, across] = values * wide[:, across]
            squares[part, :] = (parts[0] + parts[1]) + (parts[2] + parts[3])
            return carry

        lax.fori_loop(0, piece // block, gather_squares, 0)
    for step in range(1, chunks):
        weight_copy(step).start()
    for copy in table_copies[2:]:
        copy.start()
    table_copies[1].wait()
    mean = jnp.sum(squares[...], axis=-1, keepdims=True) * (1.0 / depth)
    squares[...] = jnp.broadcast_to(lax.rsqrt(mean + 1e-06), squares.shape)

    arrive()

    def chunk(step, carry):
        unit = step // HALVES
        number = step % HALVES
        half = half_of(number)
        weight_copy(step).wait()
        product = jnp.dot(raw[...], held[step], preferred_element_type=jnp.float32)
        scaling = jnp.concatenate([squares[...]] * (width // LANES), axis=1)
        hidden = (product * scaling).astype(jnp.bfloat16)
        spectrum = lax.dot_general(
            forward[...], hidden, (((1,), (1,)), ((), ())), preferred_element_type=jnp.float32
        )
        sent[unit, pl.ds(half * members, members)] = spectrum.reshape(members, slots, rows).astype(jnp.bfloat16)
        for inside in range(PLANES // HALVES):
            plane_step = number * (PLANES // HALVES) + inside
            send_plane(
                devices,
                plane_step,
                sent.at[unit],
                taken.at[unit],
                send_sem.at[unit],
                recv_sem.at[unit],
                plane_step // (PLANES - 1),
            )
        return carry

    lax.fori_loop(0, chunks, chunk, 0)
    for unit in range(units):
        pltpu.make_async_copy(sent.at[unit, me], taken.at[unit, me], own_sem.at[unit]).start()
    out_copy.start()
    last_copy.start()

    for copy in table_copies[2:]:
        copy.wait()
    zeroth_here = me % places == 0

    @pl.when(zeroth_here)
    def _():
        table[...] = special[...]

    @pl.when(jnp.logical_not(zeroth_here))
    def _():
        table[...] = usual[...]

    def turned(slot):
        a = lax.dot_general(
            grid[slot], first[...], (((0,), (0,)), ((), ())), preferred_element_type=jnp.float32
        )
        re, im = a[:, :outer], a[:, outer:]
        c, s = turn_cos[...], turn_sin[...]
        return [(re * c + im * s).astype(jnp.bfloat16), (im * c - re * s).astype(jnp.bfloat16)]

    for unit in range(units):
        pltpu.make_async_copy(sent.at[unit, me], taken.at[unit, me], own_sem.at[unit]).wait()
        wait_for(taken.at[unit], recv_sem.at[unit], devices - 1)
        for part in range(outer // devices):
            piece_of = taken[unit, :, :, part * inner : (part + 1) * inner]
            grid[:, part * devices : (part + 1) * devices, :] = jnp.swapaxes(
                piece_of.astype(jnp.float32), 0, 1
            ).astype(jnp.bfloat16)
        for pair in range(pairs):
            b = jnp.concatenate(turned(pair) + turned(pair + pairs), axis=0)
            here_table = table if pair == 0 else usual
            o = jnp.dot(here_table[...], b, preferred_element_type=jnp.float32)
            done[pair] = o[:inner]
            done[pair + pairs] = o[inner:]
        for part in range(inner // devices):
            piece_of = done[:, part * devices : (part + 1) * devices, :]
            back[unit, :, :, part * outer : (part + 1) * outer] = jnp.swapaxes(piece_of, 0, 1).astype(jnp.bfloat16)
        for step in range(PLANES):
            send_plane(
                devices,
                step,
                back.at[unit],
                landed.at[unit],
                back_sem.at[unit],
                landed_sem.at[unit, step // HALVES],
                step // (PLANES - 1),
            )
        pltpu.make_async_copy(back.at[unit, me], landed.at[unit, me], own_back_sem.at[unit]).start()

    def put_in_order(unit, half):
        parts = landed[unit, pl.ds(half * members, members)].astype(jnp.float32)
        joined = parts.reshape(width, rows).astype(jnp.bfloat16)
        return lax.dot_general(
            joined, order[...], (((0,), (0,)), ((), ())), preferred_element_type=jnp.float32
        ).astype(jnp.bfloat16)

    tile = out_width // 8
    out_copy.wait()
    for unit in range(units):
        pltpu.make_async_copy(back.at[unit, me], landed.at[unit, me], own_back_sem.at[unit]).wait()
        for number in reversed(range(HALVES)):
            wait_for(landed.at[unit], landed_sem.at[unit, number], members - number)
            half = half_of(number)
            if unit == units - 1 and number == 0:
                last[...] = put_in_order(unit, half)
                continue
            ordered[...] = put_in_order(unit, half)
            begin = pl.multiple_of((unit * HALVES + half) * width, width)
            starting = unit == 0 and number == HALVES - 1

            def add_up(index, carry):
                across = pl.ds(pl.multiple_of(index * tile, tile), tile)
                product = jnp.dot(
                    ordered[...], held_out[pl.ds(begin, width), across], preferred_element_type=jnp.float32
                )
                total[:, across] = product if starting else total[:, across] + product
                return carry

            lax.fori_loop(0, out_width // tile, add_up, 0)

    last_copy.wait()
    for unit in range(units):
        wait_for(sent.at[unit], send_sem.at[unit], devices - 1)
        wait_for(back.at[unit], back_sem.at[unit], devices - 1)


def mixer(tokens, gain, weight, out_weight, forward, tables, order, units, devices):
    rows, depth = tokens.shape
    channels = weight.shape[1]
    slots = channels // devices // units
    outer = tables[0].shape[0]
    inner = tables[1].shape[0]
    width = channels // units // HALVES
    out_width = out_weight.shape[1]
    whole = pl.BlockSpec(memory_space=pltpu.VMEM)
    hbm = pl.BlockSpec(memory_space=pltpu.HBM)
    pieces = 4
    block = 16
    small = (gain, forward, *tables, order)
    return pl.pallas_call(
        functools.partial(mixer_kernel, devices),
        out_shape=(
            pltpu.VMEM((rows, out_width), jnp.float32),
            pltpu.VMEM((rows, width), jnp.bfloat16),
            pltpu.VMEM((width, out_width), jnp.bfloat16),
        ),
        in_specs=[hbm] * (3 + len(small)),
        out_specs=(whole, whole, whole),
        scratch_shapes=[pltpu.VMEM(table.shape, table.dtype) for table in small] + [
            pltpu.VMEM((rows, depth), jnp.bfloat16),
            pltpu.VMEM((units * HALVES, depth, width), jnp.bfloat16),
            pltpu.VMEM((channels, out_width), jnp.bfloat16),
            pltpu.VMEM((block, depth), jnp.bfloat16),
            pltpu.VMEM((rows, LANES), jnp.float32),
            pltpu.VMEM((units, devices, slots, rows), jnp.bfloat16),
            pltpu.VMEM((units, devices, slots, rows), jnp.bfloat16),
            pltpu.VMEM(tables[3].shape, jnp.bfloat16),
            pltpu.VMEM((slots, outer, inner), jnp.bfloat16),
            pltpu.VMEM((slots, inner, outer), jnp.float32),
            pltpu.VMEM((units, devices, slots, rows), jnp.bfloat16),
            pltpu.VMEM((units, devices, slots, rows), jnp.bfloat16),
            pltpu.VMEM((rows, width), jnp.bfloat16),
            pltpu.SemaphoreType.DMA((pieces,)),
            pltpu.SemaphoreType.DMA((units * HALVES,)),
            pltpu.SemaphoreType.DMA,
            pltpu.SemaphoreType.DMA,
            pltpu.SemaphoreType.DMA((units,)),
            pltpu.SemaphoreType.DMA((units,)),
            pltpu.SemaphoreType.DMA((units,)),
            pltpu.SemaphoreType.DMA((units,)),
            pltpu.SemaphoreType.DMA((units,)),
            pltpu.SemaphoreType.DMA((units, HALVES)),
            pltpu.SemaphoreType.DMA((len(small),)),
        ],
        compiler_params=pltpu.CompilerParams(collective_id=0, has_side_effects=True, vmem_limit_bytes=46 << 20),
    )(*[pltpu.with_memory_space_constraint(array, pltpu.HBM) for array in (tokens, weight, out_weight, *small)])


def local(tokens, norm_gain, in_weight, out_weight):
    rows_here = tokens.shape[0]
    channels = in_weight.shape[1]
    devices = lax.axis_size(AXES)
    slots = channels // devices
    units = max(1, slots // 16)
    length = rows_here * devices
    inner = 1 << ((length.bit_length()) // 2)
    outer = length // inner

    forward, order = channel_tables(slots // units)
    several = np.eye(channels // units // HALVES // GROUP_WIDTH)
    forward = np.kron(several, forward.astype(np.float32)).astype(jnp.bfloat16)
    order = np.kron(several, order.astype(np.float32)).T.astype(jnp.bfloat16)
    tables = position_tables(outer, inner, devices)
    total, last, last_weight = mixer(
        tokens, norm_gain, in_weight, out_weight, forward, tables, order, units, devices
    )
    return (total + jnp.dot(last, last_weight, preferred_element_type=jnp.float32)).astype(jnp.bfloat16)


def solution(mesh):
    placed = (P(AXES, None), P(), P(), P())
    return jax.shard_map(
        local, mesh=mesh, in_specs=placed, out_specs=P(AXES, None), check_vma=False
    )
```

time: 70.3 us -> 58.8 us (0.84)
  Pallas kernels: 62.7 us -> 54.8 us
  matrix products: 6.08 us -> 3.28 us
  local copies, waits for them, and re-layouts: 1.25 us -> 0 us
    pallas_call x2 -> x1, Pallas kernels: 62.7 us -> 54.8 us  [mixer(): pl.pallas_call(functools.partial(mixer_kernel, devices), out_shape=(pltpu...]
    dot_general x1, matrix products: 6.08 us -> 3.28 us  [local(): jnp.dot(last, last_weight, preferred_element_type=jnp.float32)]
    unnamed x16 -> x0, local copies, waits for them, and re-layouts: 1.25 us -> none
where the time goes in v1:
time: 58.8 us; the launch traced here: 58.1 us
  Pallas kernels  54.8 us (93%)
  matrix products  3.28 us (6%)
    pallas_call x1, Pallas kernels, mixer(): pl.pallas_call(functools.partial(mixer_kernel, devices), out_shape=(pltpu...  54.8 us
    dot_general x1, matrix products, local(): jnp.dot(last, last_weight, preferred_element_type=jnp.float32)  3.28 us

profile of v1, /device:TPU:9, one launch (start us, length us, event | category | flops | bytes accessed | tf_op | source)
XLA Modules:
  0.0 58.1 jit_solution(13596025050749656336)
XLA Ops:
  0.0 54.8 %shard_map.109 = (f32[512,4096]{1,0:T(8,128)S(1)}, bf16[512,256]{1,0:T(8,128)(2,1)S(1)}, bf16[256,4096]{1,0:T(8,128)(2,1)S(1)}) custom-call(bf16[512,4096]{1,0:T(8,128)(2,1)} %tokens.1, bf16[4096,1024]{1,0:T(8,128)(2,1)} %weight.1, bf16[1024,4096]{1,0:T(8,128)(2,1)} %out_weight.1, bf16[4096]{0:T(1024)(128)(2,1)} %gain_hbm.1, ...), custom_call_target="tpu_custom_call" | custom-call | tf_op jit(solution)/shard_map/pallas_call | solution.py:373
  54.8 3.3 %add_convert_fusion = bf16[512,4096]{1,0:T(8,128)(2,1)} fusion(f32[512,4096]{1,0:T(8,128)S(1)} %get-tuple-element.8, bf16[512,256]{1,0:T(8,128)(2,1)S(1)} %get-tuple-element.9, bf16[256,4096]{1,0:T(8,128)(2,1)S(1)} %get-tuple-element.10), kind=kOutput, calls=%fused_computation | convolution fusion | flops 1077936128 | bytes 14942208 | tf_op jit(solution)/shard_map/dot_general | solution.py:430

commit v2 on v1

--- a/solution.py
+++ b/solution.py
@@ -61,6 +61,7 @@
 
 PLANES = 4
 HALVES = 2
+SPLIT = 2
 LANES = 128
 MESH = pl.DeviceIdType.MESH
 
@@ -95,15 +96,15 @@
     return lambda: pl.semaphore_wait(barrier, devices - 1)
 
 
-def send_plane(devices, step, from_ref, to_ref, send_sem, recv_sem, first):
+def send_plane(devices, step, from_ref, to_ref, send_sem, recv_sem, first, across=slice(None)):
     me, columns, per, plane, lane = here(devices)
     target_plane = turned_plane(plane, step)
 
     def send(hop, carry):
         target = target_plane * per + (lane + hop) % per
         pltpu.make_async_remote_copy(
-            src_ref=from_ref.at[target],
-            dst_ref=to_ref.at[me],
+            src_ref=from_ref.at[target, :, across],
+            dst_ref=to_ref.at[me, :, across],
             send_sem=send_sem,
             recv_sem=recv_sem,
             device_id=place_of(target, columns),
@@ -157,6 +158,7 @@
     landed,
     ordered,
     token_sem,
+    first_weight_sem,
     weight_sem,
     out_sem,
     last_sem,
@@ -172,6 +174,7 @@
     pieces = token_sem.shape[0]
     rows, depth = raw.shape
     piece = rows // pieces
+    first_piece = depth // pieces
     width = held.shape[2]
     units, _, slots, _ = sent.shape
     members = devices // HALVES
@@ -194,6 +197,13 @@
         begin = pl.multiple_of((step // HALVES * HALVES + half_of(step % HALVES)) * width, width)
         return pltpu.make_async_copy(weight.at[:, pl.ds(begin, width)], held.at[step], weight_sem.at[step])
 
+    def first_weight_copy(index):
+        part = pl.ds(index * first_piece, first_piece)
+        begin = pl.multiple_of(half_of(0) * width, width)
+        return pltpu.make_async_copy(
+            weight.at[part, pl.ds(begin, width)], held.at[0, part], first_weight_sem.at[index]
+        )
+
     out_width = out_weight.shape[1]
     far_begin = pl.multiple_of(((units - 1) * HALVES + far) * width, width)
     out_copy = pltpu.make_async_copy(out_weight, held_out, out_sem)
@@ -205,53 +215,30 @@
         pltpu.make_async_copy(a, b, table_sem.at[index]) for index, (a, b) in enumerate(zip(distant, nearby))
     ]
     table_copies[0].start()
+    ahead = pieces // SPLIT
+    for index in range(ahead):
+        token_copy(index).start()
     for index in range(pieces):
-        token_copy(index).start()
-    weight_copy(0).start()
+        first_weight_copy(index).start()
     table_copies[1].start()
     arrive = greet(devices)
 
     block = wide.shape[0]
     table_copies[0].wait()
     wide[...] = jnp.broadcast_to(gain[...].astype(jnp.float32).reshape(1, depth), wide.shape).astype(jnp.bfloat16)
-    for index in range(pieces):
-        token_copy(index).wait()
-
-        def gather_squares(number, carry):
-            part = pl.ds(pl.multiple_of(index * piece + number * block, block), block)
-            parts = [jnp.zeros((block, LANES), jnp.float32) for _ in range(4)]
-            for column in range(depth // LANES):
-                across = pl.ds(column * LANES, LANES)
-                values = raw[part, across]
-                floats = values.astype(jnp.float32)
-                parts[column % 4] = parts[column % 4] + floats * floats
-                raw[part, across] = values * wide[:, across]
-            squares[part, :] = (parts[0] + parts[1]) + (parts[2] + parts[3])
-            return carry
-
-        lax.fori_loop(0, piece // block, gather_squares, 0)
-    for step in range(1, chunks):
-        weight_copy(step).start()
-    for copy in table_copies[2:]:
-        copy.start()
-    table_copies[1].wait()
-    mean = jnp.sum(squares[...], axis=-1, keepdims=True) * (1.0 / depth)
-    squares[...] = jnp.broadcast_to(lax.rsqrt(mean + 1e-06), squares.shape)
-
-    arrive()
-
-    def chunk(step, carry):
-        unit = step // HALVES
-        number = step % HALVES
+
+    def give_out(unit, number, part, product):
         half = half_of(number)
-        weight_copy(step).wait()
-        product = jnp.dot(raw[...], held[step], preferred_element_type=jnp.float32)
-        scaling = jnp.concatenate([squares[...]] * (width // LANES), axis=1)
+        scaling = jnp.concatenate([squares[part, :]] * (width // LANES), axis=1)
         hidden = (product * scaling).astype(jnp.bfloat16)
         spectrum = lax.dot_general(
             forward[...], hidden, (((1,), (1,)), ((), ())), preferred_element_type=jnp.float32
         )
-        sent[unit, pl.ds(half * members, members)] = spectrum.reshape(members, slots, rows).astype(jnp.bfloat16)
+        sent[unit, pl.ds(half * members, members), :, part] = spectrum.reshape(
+            members, slots, part.size
+        ).astype(jnp.bfloat16)
+
+    def send_out(unit, number, part):
         for inside in range(PLANES // HALVES):
             plane_step = number * (PLANES // HALVES) + inside
             send_plane(
@@ -262,10 +249,56 @@
                 send_sem.at[unit],
                 recv_sem.at[unit],
                 plane_step // (PLANES - 1),
+                part,
             )
+
+    def gather_squares(number, carry):
+        part = pl.ds(pl.multiple_of(number * block, block), block)
+        parts = [jnp.zeros((block, LANES), jnp.float32) for _ in range(4)]
+        for column in range(depth // LANES):
+            across = pl.ds(column * LANES, LANES)
+            values = raw[part, across]
+            floats = values.astype(jnp.float32)
+            parts[column % 4] = parts[column % 4] + floats * floats
+            raw[part, across] = values * wide[:, across]
+        squares[part, :] = (parts[0] + parts[1]) + (parts[2] + parts[3])
         return carry
 
-    lax.fori_loop(0, chunks, chunk, 0)
+    begun = rows // SPLIT
+    for stage in range(SPLIT):
+        part = pl.ds(stage * begun, begun)
+        for index in range(stage * ahead, (stage + 1) * ahead):
+            token_copy(index).wait()
+            if stage < SPLIT - 1:
+                token_copy(index + ahead).start()
+            lax.fori_loop(index * piece // block, (index + 1) * piece // block, gather_squares, 0)
+        mean = jnp.sum(squares[part, :], axis=-1, keepdims=True) * (1.0 / depth)
+        squares[part, :] = jnp.broadcast_to(lax.rsqrt(mean + 1e-06), (begun, LANES))
+        if stage == 0:
+            for index in range(pieces):
+                first_weight_copy(index).wait()
+            table_copies[1].wait()
+        if stage == SPLIT - 1:
+            for step in range(1, chunks):
+                weight_copy(step).start()
+            for copy in table_copies[2:]:
+                copy.start()
+        give_out(0, 0, part, jnp.dot(raw[part, :], held[0], preferred_element_type=jnp.float32))
+        if stage == 0:
+            arrive()
+        send_out(0, 0, part)
+
+    everything = pl.ds(0, rows)
+
+    def chunk(step, carry):
+        unit = step // HALVES
+        number = step % HALVES
+        weight_copy(step).wait()
+        give_out(unit, number, everything, jnp.dot(raw[...], held[step], preferred_element_type=jnp.float32))
+        send_out(unit, number, everything)
+        return carry
+
+    lax.fori_loop(1, chunks, chunk, 0)
     for unit in range(units):
         pltpu.make_async_copy(sent.at[unit, me], taken.at[unit, me], own_sem.at[unit]).start()
     out_copy.start()
@@ -394,6 +427,7 @@
             pltpu.VMEM((units, devices, slots, rows), jnp.bfloat16),
             pltpu.VMEM((rows, width), jnp.bfloat16),
             pltpu.SemaphoreType.DMA((pieces,)),
+            pltpu.SemaphoreType.DMA((pieces,)),
             pltpu.SemaphoreType.DMA((units * HALVES,)),
             pltpu.SemaphoreType.DMA,
             pltpu.SemaphoreType.DMA,
@@ -409,6 +443,40 @@
     )(*[pltpu.with_memory_space_constraint(array, pltpu.HBM) for array in (tokens, weight, out_weight, *small)])
 
 
+def finish_kernel(total, last, last_weight, out, staged, sems):
+    tiles = sems.shape[0]
+    tile = staged.shape[1] // tiles
+
+    def store(index):
+        across = pl.ds(index * tile, tile)
+        return pltpu.make_async_copy(staged.at[:, across], out.at[:, across], sems.at[index])
+
+    for index in range(tiles):
+        across = pl.ds(index * tile, tile)
+        product = jnp.dot(last[...], last_weight[:, across], preferred_element_type=jnp.float32)
+        staged[:, across] = (total[:, across] + product).astype(jnp.bfloat16)
+        store(index).start()
+    for index in range(tiles):
+        store(index).wait()
+
+
+def finish(total, last, last_weight):
+    rows, out_width = total.shape
+    tiles = 8
+    whole = pl.BlockSpec(memory_space=pltpu.VMEM)
+    return pl.pallas_call(
+        finish_kernel,
+        out_shape=pltpu.HBM((rows, out_width), jnp.bfloat16),
+        in_specs=[whole] * 3,
+        out_specs=pl.BlockSpec(memory_space=pltpu.HBM),
+        scratch_shapes=[
+            pltpu.VMEM((rows, out_width), jnp.bfloat16),
+            pltpu.SemaphoreType.DMA((tiles,)),
+        ],
+        compiler_params=pltpu.CompilerParams(vmem_limit_bytes=20 << 20),
+    )(total, last, last_weight)
+
+
 def local(tokens, norm_gain, in_weight, out_weight):
     rows_here = tokens.shape[0]
     channels = in_weight.shape[1]
@@ -427,7 +495,7 @@
     total, last, last_weight = mixer(
         tokens, norm_gain, in_weight, out_weight, forward, tables, order, units, devices
     )
-    return (total + jnp.dot(last, last_weight, preferred_element_type=jnp.float32)).astype(jnp.bfloat16)
+    return finish(total, last, last_weight)
 
 
 def solution(mesh):

time: 58.8 us -> 56 us (0.952)
  matrix products: 3.28 us -> 0 us
  Pallas kernels: 54.8 us -> 55.7 us
    dot_general x1 -> x0, matrix products: 3.28 us -> none  [local(): jnp.dot(last, last_weight, preferred_element_type=jnp.float32)]
    pallas_call x0 -> x1, Pallas kernels: none -> 2.38 us  [finish(): pl.pallas_call(finish_kernel, out_shape=pltpu.HBM((rows, out_width), jnp....]
    pallas_call x1, Pallas kernels: 54.8 us -> 53.3 us  [mixer(): pl.pallas_call(functools.partial(mixer_kernel, devices), out_shape=(pltpu...]
where the time goes in v2:
time: 56 us; the launch traced here: 55.7 us
  Pallas kernels  55.7 us (99%)
    pallas_call x1, Pallas kernels, mixer(): pl.pallas_call(functools.partial(mixer_kernel, devices), out_shape=(pltpu...  53.3 us
    pallas_call x1, Pallas kernels, finish(): pl.pallas_call(finish_kernel, out_shape=pltpu.HBM((rows, out_width), jnp....  2.38 us

profile of v2, /device:TPU:9, one launch (start us, length us, event | category | flops | bytes accessed | tf_op | source)
XLA Modules:
  0.0 55.7 jit_solution(6923515593956998140)
XLA Ops:
  0.0 53.3 %shard_map.109 = (f32[512,4096]{1,0:T(8,128)S(1)}, bf16[512,256]{1,0:T(8,128)(2,1)S(1)}, bf16[256,4096]{1,0:T(8,128)(2,1)S(1)}) custom-call(bf16[512,4096]{1,0:T(8,128)(2,1)} %tokens.1, bf16[4096,1024]{1,0:T(8,128)(2,1)} %weight.1, bf16[1024,4096]{1,0:T(8,128)(2,1)} %out_weight.1, bf16[4096]{0:T(1024)(128)(2,1)} %gain_hbm.1, ...), custom_call_target="tpu_custom_call" | custom-call | tf_op jit(solution)/shard_map/pallas_call | solution.py:406
  53.4 2.4 %shard_map.110 = bf16[512,4096]{1,0:T(8,128)(2,1)} custom-call(f32[512,4096]{1,0:T(8,128)S(1)} %get-tuple-element.8.total, bf16[512,256]{1,0:T(8,128)(2,1)S(1)} %get-tuple-element.9.last, bf16[256,4096]{1,0:T(8,128)(2,1)S(1)} %get-tuple-element.10.last_weight), custom_call_target="tpu_custom_call" | custom-call | tf_op jit(solution)/shard_map/pallas_call | solution.py:467

commit v3 on v2

--- a/solution.py
+++ b/solution.py
@@ -61,7 +61,6 @@
 
 PLANES = 4
 HALVES = 2
-SPLIT = 2
 LANES = 128
 MESH = pl.DeviceIdType.MESH
 
@@ -215,13 +214,11 @@
         pltpu.make_async_copy(a, b, table_sem.at[index]) for index, (a, b) in enumerate(zip(distant, nearby))
     ]
     table_copies[0].start()
-    ahead = pieces // SPLIT
-    for index in range(ahead):
-        token_copy(index).start()
+    token_copy(0).start()
+    arrive = greet(devices)
     for index in range(pieces):
         first_weight_copy(index).start()
     table_copies[1].start()
-    arrive = greet(devices)
 
     block = wide.shape[0]
     table_copies[0].wait()
@@ -264,21 +261,23 @@
         squares[part, :] = (parts[0] + parts[1]) + (parts[2] + parts[3])
         return carry
 
-    begun = rows // SPLIT
-    for stage in range(SPLIT):
-        part = pl.ds(stage * begun, begun)
-        for index in range(stage * ahead, (stage + 1) * ahead):
+    stages = [(index, index + 1) for index in range(pieces)]
+    for stage, (begin, end) in enumerate(stages):
+        begun = (end - begin) * piece
+        part = pl.ds(begin * piece, begun)
+        for index in range(begin, end):
             token_copy(index).wait()
-            if stage < SPLIT - 1:
-                token_copy(index + ahead).start()
-            lax.fori_loop(index * piece // block, (index + 1) * piece // block, gather_squares, 0)
+            if index == 0:
+                for later in range(1, pieces):
+                    token_copy(later).start()
+            lax.fori_loop(index * piece // block, (index + 1) * piece // block, gather_squares, 0, unroll=2)
         mean = jnp.sum(squares[part, :], axis=-1, keepdims=True) * (1.0 / depth)
         squares[part, :] = jnp.broadcast_to(lax.rsqrt(mean + 1e-06), (begun, LANES))
         if stage == 0:
             for index in range(pieces):
                 first_weight_copy(index).wait()
             table_copies[1].wait()
-        if stage == SPLIT - 1:
+        if stage == len(stages) - 1:
             for step in range(1, chunks):
                 weight_copy(step).start()
             for copy in table_copies[2:]:

time: 56 us -> 55.1 us (0.984)
  Pallas kernels: 55.7 us -> 54.8 us
    pallas_call x1, Pallas kernels: 53.3 us -> 52.5 us  [mixer(): pl.pallas_call(functools.partial(mixer_kernel, devices), out_shape=(pltpu...]
where the time goes in v3:
time: 55.1 us; the launch traced here: 54.9 us
  Pallas kernels  54.8 us (99%)
    pallas_call x1, Pallas kernels, mixer(): pl.pallas_call(functools.partial(mixer_kernel, devices), out_shape=(pltpu...  52.5 us
    pallas_call x1, Pallas kernels, finish(): pl.pallas_call(finish_kernel, out_shape=pltpu.HBM((rows, out_width), jnp....  2.38 us

profile of v3, /device:TPU:9, one launch (start us, length us, event | category | flops | bytes accessed | tf_op | source)
XLA Modules:
  0.0 54.9 jit_solution(4037067759185647591)
XLA Ops:
  0.0 52.5 %shard_map.109 = (f32[512,4096]{1,0:T(8,128)S(1)}, bf16[512,256]{1,0:T(8,128)(2,1)S(1)}, bf16[256,4096]{1,0:T(8,128)(2,1)S(1)}) custom-call(bf16[512,4096]{1,0:T(8,128)(2,1)} %tokens.1, bf16[4096,1024]{1,0:T(8,128)(2,1)} %weight.1, bf16[1024,4096]{1,0:T(8,128)(2,1)} %out_weight.1, bf16[4096]{0:T(1024)(128)(2,1)} %gain_hbm.1, ...), custom_call_target="tpu_custom_call" | custom-call | tf_op jit(solution)/shard_map/pallas_call | solution.py:405
  52.5 2.4 %shard_map.110 = bf16[512,4096]{1,0:T(8,128)(2,1)} custom-call(f32[512,4096]{1,0:T(8,128)S(1)} %get-tuple-element.8.total, bf16[512,256]{1,0:T(8,128)(2,1)S(1)} %get-tuple-element.9.last, bf16[256,4096]{1,0:T(8,128)(2,1)S(1)} %get-tuple-element.10.last_weight), custom_call_target="tpu_custom_call" | custom-call | tf_op jit(solution)/shard_map/pallas_call | solution.py:466

commit v4 on v3

--- a/solution.py
+++ b/solution.py
@@ -1,4 +1,5 @@
 import functools
+import itertools
 import math
 
 import jax
@@ -61,6 +62,7 @@
 
 PLANES = 4
 HALVES = 2
+CUTS = 2
 LANES = 128
 MESH = pl.DeviceIdType.MESH
 
@@ -114,9 +116,38 @@
     lax.fori_loop(first, per, send, 0)
 
 
+def send_far(devices, place, lanes, from_ref, to_ref, send_sem, recv_sem, across=slice(None)):
+    me, columns, per, plane, lane = here(devices)
+    low = plane // 2
+    target_plane = (1 - low) * (2 + place) + low * ((plane % 2 + place) % 2)
+    quarter = per // 4
+
+    def send(hop, carry):
+        spot = (lane + hop) % (per // 2)
+        target_lane = (1 - lanes) * (spot + spot // quarter * 2 * quarter) + lanes * (quarter + spot)
+        target = target_plane * per + target_lane
+        pltpu.make_async_remote_copy(
+            src_ref=from_ref.at[target, :, across],
+            dst_ref=to_ref.at[me, :, across],
+            send_sem=send_sem,
+            recv_sem=recv_sem,
+            device_id=place_of(target, columns),
+            device_id_type=MESH,
+        ).start()
+        return carry
+
+    lax.fori_loop(0, per // 2, send, 0)
+
+
 def wait_for(ref, sem, count):
     part = ref.at[pl.ds(0, count)]
     pltpu.make_async_copy(part, part, sem).wait()
+
+
+def put_in_order(joined, order):
+    return lax.dot_general(
+        joined, order[...], (((0,), (0,)), ((), ())), preferred_element_type=jnp.float32
+    ).astype(jnp.bfloat16)
 
 
 def mixer_kernel(
@@ -135,6 +166,8 @@
     total,
     last,
     last_weight,
+    early,
+    order,
     gain,
     forward,
     first,
@@ -142,7 +175,6 @@
     turn_sin,
     usual,
     special,
-    order,
     raw,
     held,
     held_out,
@@ -184,6 +216,7 @@
     outer = first.shape[0]
     inner = turn_cos.shape[0]
     chunks = units * HALVES
+    cut_rows = rows // CUTS
 
     def token_copy(index):
         part = pl.ds(index * piece, piece)
@@ -340,50 +373,68 @@
         for part in range(inner // devices):
             piece_of = done[:, part * devices : (part + 1) * devices, :]
             back[unit, :, :, part * outer : (part + 1) * outer] = jnp.swapaxes(piece_of, 0, 1).astype(jnp.bfloat16)
-        for step in range(PLANES):
+        last_unit = unit == units - 1
+        for place, cut, lanes in itertools.product(range(2), range(CUTS if last_unit else 1), range(2)):
+            send_far(
+                devices,
+                place,
+                lanes,
+                back.at[unit],
+                landed.at[unit],
+                back_sem.at[unit],
+                landed_sem.at[unit, cut],
+                pl.ds(cut * cut_rows, cut_rows) if last_unit else slice(None),
+            )
+        for step in range(HALVES, PLANES):
             send_plane(
                 devices,
                 step,
                 back.at[unit],
                 landed.at[unit],
                 back_sem.at[unit],
-                landed_sem.at[unit, step // HALVES],
+                landed_sem.at[unit, CUTS],
                 step // (PLANES - 1),
             )
         pltpu.make_async_copy(back.at[unit, me], landed.at[unit, me], own_back_sem.at[unit]).start()
 
-    def put_in_order(unit, half):
-        parts = landed[unit, pl.ds(half * members, members)].astype(jnp.float32)
-        joined = parts.reshape(width, rows).astype(jnp.bfloat16)
-        return lax.dot_general(
-            joined, order[...], (((0,), (0,)), ((), ())), preferred_element_type=jnp.float32
-        ).astype(jnp.bfloat16)
-
-    tile = out_width // 8
+    def joined(unit, half, across):
+        parts = landed[unit, pl.ds(half * members, members), :, across].astype(jnp.float32)
+        return parts.reshape(width, parts.shape[2]).astype(jnp.bfloat16)
+
+    tile = out_width // 4
+    tiles = out_width // tile
     out_copy.wait()
     for unit in range(units):
         pltpu.make_async_copy(back.at[unit, me], landed.at[unit, me], own_back_sem.at[unit]).wait()
         for number in reversed(range(HALVES)):
-            wait_for(landed.at[unit], landed_sem.at[unit, number], members - number)
             half = half_of(number)
-            if unit == units - 1 and number == 0:
-                last[...] = put_in_order(unit, half)
-                continue
-            ordered[...] = put_in_order(unit, half)
             begin = pl.multiple_of((unit * HALVES + half) * width, width)
+            closing = unit == units - 1 and number == 0
             starting = unit == 0 and number == HALVES - 1
+            part = pl.ds(0, cut_rows) if closing else pl.ds(0, rows)
+            if closing:
+                wait_for(landed.at[unit, :, :, part], landed_sem.at[unit, 0], members)
+            else:
+                wait_for(landed.at[unit], landed_sem.at[unit, CUTS * number], members - number)
+            ordered[part, :] = put_in_order(joined(unit, half, part), order)
 
             def add_up(index, carry):
                 across = pl.ds(pl.multiple_of(index * tile, tile), tile)
                 product = jnp.dot(
-                    ordered[...], held_out[pl.ds(begin, width), across], preferred_element_type=jnp.float32
+                    ordered[part, :], held_out[pl.ds(begin, width), across], preferred_element_type=jnp.float32
                 )
-                total[:, across] = product if starting else total[:, across] + product
+                if closing:
+                    early[:, across] = (total[part, across] + product).astype(jnp.bfloat16)
+                else:
+                    total[:, across] = product if starting else total[:, across] + product
                 return carry
 
-            lax.fori_loop(0, out_width // tile, add_up, 0)
+            lax.fori_loop(0, tiles, add_up, 0)
 
     last_copy.wait()
+    rest = pl.ds(cut_rows, cut_rows)
+    wait_for(landed.at[units - 1, :, :, rest], landed_sem.at[units - 1, 1], members)
+    last[...] = joined(units - 1, half_of(0), rest)
     for unit in range(units):
         wait_for(sent.at[unit], send_sem.at[unit], devices - 1)
         wait_for(back.at[unit], back_sem.at[unit], devices - 1)
@@ -406,12 +457,14 @@
         functools.partial(mixer_kernel, devices),
         out_shape=(
             pltpu.VMEM((rows, out_width), jnp.float32),
-            pltpu.VMEM((rows, width), jnp.bfloat16),
+            pltpu.VMEM((width, rows // CUTS), jnp.bfloat16),
             pltpu.VMEM((width, out_width), jnp.bfloat16),
+            pltpu.VMEM((rows // CUTS, out_width), jnp.bfloat16),
+            pltpu.VMEM(order.shape, order.dtype),
         ),
         in_specs=[hbm] * (3 + len(small)),
-        out_specs=(whole, whole, whole),
-        scratch_shapes=[pltpu.VMEM(table.shape, table.dtype) for table in small] + [
+        out_specs=(whole,) * 5,
+        scratch_shapes=[pltpu.VMEM(table.shape, table.dtype) for table in small[:-1]] + [
             pltpu.VMEM((rows, depth), jnp.bfloat16),
             pltpu.VMEM((units * HALVES, depth, width), jnp.bfloat16),
             pltpu.VMEM((channels, out_width), jnp.bfloat16),
@@ -435,45 +488,53 @@
             pltpu.SemaphoreType.DMA((units,)),
             pltpu.SemaphoreType.DMA((units,)),
             pltpu.SemaphoreType.DMA((units,)),
-            pltpu.SemaphoreType.DMA((units, HALVES)),
+            pltpu.SemaphoreType.DMA((units, CUTS + 1)),
             pltpu.SemaphoreType.DMA((len(small),)),
         ],
         compiler_params=pltpu.CompilerParams(collective_id=0, has_side_effects=True, vmem_limit_bytes=46 << 20),
     )(*[pltpu.with_memory_space_constraint(array, pltpu.HBM) for array in (tokens, weight, out_weight, *small)])
 
 
-def finish_kernel(total, last, last_weight, out, staged, sems):
+def finish_kernel(total, last, last_weight, early, order, out, staged, ordered, sems, early_sem):
     tiles = sems.shape[0]
-    tile = staged.shape[1] // tiles
+    begin, out_width = staged.shape
+    tile = out_width // tiles
+    early_copy = pltpu.make_async_copy(early, out.at[pl.ds(0, begin)], early_sem)
+    early_copy.start()
+    ordered[...] = put_in_order(last[...], order)
 
     def store(index):
         across = pl.ds(index * tile, tile)
-        return pltpu.make_async_copy(staged.at[:, across], out.at[:, across], sems.at[index])
+        return pltpu.make_async_copy(staged.at[:, across], out.at[pl.ds(begin, begin), across], sems.at[index])
 
     for index in range(tiles):
         across = pl.ds(index * tile, tile)
-        product = jnp.dot(last[...], last_weight[:, across], preferred_element_type=jnp.float32)
-        staged[:, across] = (total[:, across] + product).astype(jnp.bfloat16)
+        product = jnp.dot(ordered[...], last_weight[:, across], preferred_element_type=jnp.float32)
+        staged[:, across] = (total[pl.ds(begin, begin), across] + product).astype(jnp.bfloat16)
         store(index).start()
+    early_copy.wait()
     for index in range(tiles):
         store(index).wait()
 
 
-def finish(total, last, last_weight):
+def finish(total, last, last_weight, early, order):
     rows, out_width = total.shape
-    tiles = 8
+    width = last_weight.shape[0]
+    tiles = 4
     whole = pl.BlockSpec(memory_space=pltpu.VMEM)
     return pl.pallas_call(
         finish_kernel,
         out_shape=pltpu.HBM((rows, out_width), jnp.bfloat16),
-        in_specs=[whole] * 3,
+        in_specs=[whole] * 5,
         out_specs=pl.BlockSpec(memory_space=pltpu.HBM),
         scratch_shapes=[
-            pltpu.VMEM((rows, out_width), jnp.bfloat16),
+            pltpu.VMEM((rows // CUTS, out_width), jnp.bfloat16),
+            pltpu.VMEM((rows // CUTS, width), jnp.bfloat16),
             pltpu.SemaphoreType.DMA((tiles,)),
+            pltpu.SemaphoreType.DMA,
         ],
         compiler_params=pltpu.CompilerParams(vmem_limit_bytes=20 << 20),
-    )(total, last, last_weight)
+    )(total, last, last_weight, early, order)
 
 
 def local(tokens, norm_gain, in_weight, out_weight):
@@ -491,10 +552,8 @@
     forward = np.kron(several, forward.astype(np.float32)).astype(jnp.bfloat16)
     order = np.kron(several, order.astype(np.float32)).T.astype(jnp.bfloat16)
     tables = position_tables(outer, inner, devices)
-    total, last, last_weight = mixer(
-        tokens, norm_gain, in_weight, out_weight, forward, tables, order, units, devices
-    )
-    return finish(total, last, last_weight)
+    parts = mixer(tokens, norm_gain, in_weight, out_weight, forward, tables, order, units, devices)
+    return finish(*parts)
 
 
 def solution(mesh):

time: 55.1 us -> 54.8 us (level)
  no operation moved by 1% of the time
where the time goes in v4:
time: 54.8 us; the launch traced here: 54.6 us
  Pallas kernels  54.6 us (100%)
    pallas_call x1, Pallas kernels, mixer(): pl.pallas_call(functools.partial(mixer_kernel, devices), out_shape=(pltpu...  52.5 us
    pallas_call x1, Pallas kernels, finish(): pl.pallas_call(finish_kernel, out_shape=pltpu.HBM((rows, out_width), jnp....  2.06 us

profile of v4, /device:TPU:9, one launch (start us, length us, event | category | flops | bytes accessed | tf_op | source)
XLA Modules:
  0.0 54.6 jit_solution(13403827298050990458)
XLA Ops:
  0.0 52.5 %shard_map.109 = (f32[512,4096]{1,0:T(8,128)S(1)}, bf16[256,256]{1,0:T(8,128)(2,1)S(1)}, bf16[256,4096]{1,0:T(8,128)(2,1)S(1)}, bf16[256,4096]{1,0:T(8,128)(2,1)S(1)}, bf16[256,256]{1,0:T(8,128)(2,1)S(1)}) custom-call(bf16[512,4096]{1,0:T(8,128)(2,1)} %tokens.1, bf16[4096,1024]{1,0:T(8,128)(2,1)} %weight.1, bf16[1024,4096]{1,0:T(8,128)(2,1)} %out_weight.1, ...), custom_call_target="tpu_custom_call" | custom-call | tf_op jit(solution)/shard_map/pallas_call | solution.py:456
  52.5 2.1 %shard_map.110 = bf16[512,4096]{1,0:T(8,128)(2,1)} custom-call(f32[512,4096]{1,0:T(8,128)S(1)} %get-tuple-element.10.total, bf16[256,256]{1,0:T(8,128)(2,1)S(1)} %get-tuple-element.11.last, bf16[256,4096]{1,0:T(8,128)(2,1)S(1)} %get-tuple-element.12.last_weight, bf16[256,4096]{1,0:T(8,128)(2,1)S(1)} %get-tuple-element.13.early, ...), custom_call_target="tpu_custom_call" | custom-call | tf_op jit(solution)/shard_map/pallas_call | solution.py:525

commit v5 on v4

--- a/solution.py
+++ b/solution.py
@@ -37,6 +37,12 @@
     return forward.astype(jnp.bfloat16), order.astype(jnp.bfloat16)
 
 
+def high_low(table, axis):
+    high = table.astype(jnp.bfloat16)
+    low = (table - high.astype(np.float64)).astype(jnp.bfloat16)
+    return np.concatenate([high, low], axis=axis)
+
+
 def position_tables(outer, inner, devices):
     length = outer * inner
     k1 = np.arange(outer)
@@ -52,11 +58,11 @@
     usual = np.block([[c, s, -s, c], [c, s, s, -c]])
     zeroth = np.block([[c, s, z, z], [z, z, c, s]])
     return (
-        first.astype(jnp.bfloat16),
+        high_low(first, 1),
         np.cos(turn).astype(np.float32),
         np.sin(turn).astype(np.float32),
-        usual.astype(jnp.bfloat16),
-        zeroth.astype(jnp.bfloat16),
+        high_low(usual, 0),
+        high_low(zeroth, 0),
     )
 
 
@@ -352,6 +358,7 @@
         a = lax.dot_general(
             grid[slot], first[...], (((0,), (0,)), ((), ())), preferred_element_type=jnp.float32
         )
+        a = a[:, : 2 * outer] + a[:, 2 * outer :]
         re, im = a[:, :outer], a[:, outer:]
         c, s = turn_cos[...], turn_sin[...]
         return [(re * c + im * s).astype(jnp.bfloat16), (im * c - re * s).astype(jnp.bfloat16)]
@@ -368,6 +375,7 @@
             b = jnp.concatenate(turned(pair) + turned(pair + pairs), axis=0)
             here_table = table if pair == 0 else usual
             o = jnp.dot(here_table[...], b, preferred_element_type=jnp.float32)
+            o = o[: 2 * inner] + o[2 * inner :]
             done[pair] = o[:inner]
             done[pair + pairs] = o[inner:]
         for part in range(inner // devices):

time: 54.8 us -> 55 us (level)
  no operation moved by 1% of the time
where the time goes in v5:
time: 55 us; the launch traced here: 54.8 us
  Pallas kernels  54.8 us (100%)
    pallas_call x1, Pallas kernels, mixer(): pl.pallas_call(functools.partial(mixer_kernel, devices), out_shape=(pltpu...  52.7 us
    pallas_call x1, Pallas kernels, finish(): pl.pallas_call(finish_kernel, out_shape=pltpu.HBM((rows, out_width), jnp....  2.06 us

profile of v5, /device:TPU:9, one launch (start us, length us, event | category | flops | bytes accessed | tf_op | source)
XLA Modules:
  0.0 54.8 jit_solution(17132051720421511135)
XLA Ops:
  0.0 52.7 %shard_map.109 = (f32[512,4096]{1,0:T(8,128)S(1)}, bf16[256,256]{1,0:T(8,128)(2,1)S(1)}, bf16[256,4096]{1,0:T(8,128)(2,1)S(1)}, bf16[256,4096]{1,0:T(8,128)(2,1)S(1)}, bf16[256,256]{1,0:T(8,128)(2,1)S(1)}) custom-call(bf16[512,4096]{1,0:T(8,128)(2,1)} %tokens.1, bf16[4096,1024]{1,0:T(8,128)(2,1)} %weight.1, bf16[1024,4096]{1,0:T(8,128)(2,1)} %out_weight.1, ...), custom_call_target="tpu_custom_call" | custom-call | tf_op jit(solution)/shard_map/pallas_call | solution.py:464
  52.7 2.1 %shard_map.110 = bf16[512,4096]{1,0:T(8,128)(2,1)} custom-call(f32[512,4096]{1,0:T(8,128)S(1)} %get-tuple-element.10.total, bf16[256,256]{1,0:T(8,128)(2,1)S(1)} %get-tuple-element.11.last, bf16[256,4096]{1,0:T(8,128)(2,1)S(1)} %get-tuple-element.12.last_weight, bf16[256,4096]{1,0:T(8,128)(2,1)S(1)} %get-tuple-element.13.early, ...), custom_call_target="tpu_custom_call" | custom-call | tf_op jit(solution)/shard_map/pallas_call | solution.py:533
